TPU v7x, 256 devices: a 4x2x16 block of a 4x16x16 slice. The times are simulated.
256 devices in a mesh: grp: 2 (over y), sp: 32 (over z, core), tp: 4 (over x).
Axes of the slice: x: 4, y: 2, z: 16, core: 2. Of those that a mesh axis runs over, the one named last changes fastest.
The devices are a block of a 4x16x16 slice.
Arguments:
- ssm_input: bfloat16 [8192, 1024], P(('grp', 'sp'), 'tp'), parts along dimension 0, may hold values from -6 to 6
- residual_in: bfloat16 [8192, 2048], P(('grp', 'sp')), parts along dimension 0, may hold values from -4 to 4
- log_step: float32 [64], P('tp'), may hold values from -6.91 to -2.3
- decay_real: float32 [64, 64], P('tp'), may hold values from -34 to 0, as said below
- freq: float32 [64, 64], P('tp'), may hold values from 0.5 to 8
- in_real: float32 [64, 64, 16], P('tp'), may hold values from -1 to 1
- in_imag: float32 [64, 64, 16], P('tp'), may hold values from -1 to 1
- out_real: float32 [64, 16, 64], P('tp'), may hold values from -0.5 to 0.5
- out_imag: float32 [64, 16, 64], P('tp'), may hold values from -0.5 to 0.5
- skip: float32 [1024], P('tp'), may hold values from -3 to 3
- w_glu: bfloat16 [1024, 1024], replicated, may hold values from -0.1875 to 0.1875
- b_glu: float32 [1024], replicated, may hold values from -3 to 3
- w_branch: bfloat16 [1024, 2048], replicated, may hold values from -0.1875 to 0.1875
- norm_gain: float32 [2048], replicated, may hold values from 0.1 to 1.9
- w_gate: bfloat16 [2048, 5632], P('sp', 'tp'), may hold values from -0.125 to 0.125
- w_up: bfloat16 [2048, 5632], P('sp', 'tp'), may hold values from -0.125 to 0.125
- w_down: bfloat16 [5632, 2048], P('tp', 'sp'), may hold values from -0.078125 to 0.078125
Outputs:
- mixed: bfloat16 [8192, 2048], P(('grp', 'sp', 'tp')), parts along dimension 0
There are 2 independent parts, one for each index of `grp`. A program takes and returns all parts, laid end to end along the dimension named above; an argument that names none is the same for every part. Nothing has to cross between parts.
Inputs may be any that keep to these rules, and one draw needn't show every extreme that they name: `decay_real`: negative in every entry.
All inputs are finite; a program needn't handle non-finite values.
Results may differ from a plain program's by a relative error of at most 0.015.
Values may be sent and summed in bfloat16 or wider, within the bound.
A program may use at most 128 MiB of HBM per device.

v0:
```python
import math
import jax
import jax.numpy as jnp
from jax import lax
from jax.sharding import Mesh
from jax.sharding import PartitionSpec as P

SP = ("sp_0", "sp_1")
GRP_SP = ("grp", "sp_0", "sp_1")
GRP_SP_TP = ("grp", "sp_0", "sp_1", "tp")
EPS = 1e-06


def sent_together(arrays, axis, dim, along):
    ends, at = ([], 0)
    for a in arrays[:-1]:
        at += a.shape[along]
        ends.append(at)
    both = jnp.concatenate(arrays, axis=along)
    return tuple(jnp.split(lax.all_gather(both, axis, axis=dim, tiled=True), ends, axis=along))


def neutral_like(shard, identity):
    return jax.tree.map(
        lambda a, e: jnp.broadcast_to(jnp.asarray(e, a.dtype), a.shape), shard, identity
    )


def all_in_one(shard, axis):
    leaves = jax.tree.leaves(shard)
    turns = sorted(range(len(leaves)), key=lambda k: -leaves[k].size)
    width = (1, *leaves[turns[0]].shape)[-1]
    lines = [
        jnp.pad(leaves[k].reshape(-1), (0, -leaves[k].size % width)).reshape(-1, width)
        for k in turns
    ]
    both, at, found = (lax.all_gather(jnp.concatenate(lines), axis), 0, {})
    for k, line in zip(turns, lines):
        piece = both[:, at : at + len(line)].reshape(len(both), -1)
        found[k] = piece[:, : leaves[k].size].reshape(-1, *leaves[k].shape)
        at += len(line)
    numbers = iter(range(len(leaves)))
    return jax.tree.map(lambda _: found[next(numbers)], shard)


def entering_2(shard, axes, combine, identity):
    before = start = neutral_like(shard, identity)
    so_far = shard
    for axis in reversed(axes):
        count, place = (lax.axis_size(axis), lax.axis_index(axis))
        pieces = all_in_one(so_far, axis)
        inside, so_far = (start, start)
        for k in range(count):
            passed = k < place
            so_far = combine(so_far, jax.tree.map(lambda part: part[k], pieces))
            inside = jax.tree.map(lambda new, old: jnp.where(passed, new, old), so_far, inside)
        before = combine(inside, before)
    return before


def sent_to_all(shard, axis):
    count = lax.axis_size(axis)
    return lax.all_to_all(
        jnp.broadcast_to(shard[None], (count, *shard.shape)), axis, 0, 0, tiled=True
    )


def in_order(pieces, dim):
    dims = list(pieces.shape[1:])
    dims[dim] *= pieces.shape[0]
    return jnp.moveaxis(pieces, 0, dim).reshape(dims)


def gather_directly(shard, axis, dim):
    pieces = sent_to_all(shard, axis)
    return in_order(pieces, dim)


def cut_along(shard, dim, count):
    dims = shard.shape
    pieces = shard.reshape(*dims[:dim], count, dims[dim] // count, *dims[dim + 1 :])
    return jnp.moveaxis(pieces, dim, 0)


def summed_on_arrival(shard, axis, dim):
    pieces = cut_along(shard, dim, lax.axis_size(axis))
    arrived = lax.all_to_all(pieces, axis, split_axis=0, concat_axis=0, tiled=True)
    return arrived.astype(jnp.float32).sum(axis=0)


def discretize(log_step, decay_real, freq, in_real, in_imag):
    step_size = jnp.exp(log_step)[:, None]
    magnitude = jnp.exp(decay_real * step_size)
    abar_re = magnitude * jnp.cos(freq * step_size)
    abar_im = magnitude * jnp.sin(freq * step_size)
    denominator = decay_real * decay_real + freq * freq
    less_re = abar_re - 1.0
    hold_re = ((less_re * decay_real + abar_im * freq) / denominator)[..., None]
    hold_im = ((abar_im * decay_real - less_re * freq) / denominator)[..., None]
    bbar_re = hold_re * in_real - hold_im * in_imag
    bbar_im = hold_re * in_imag + hold_im * in_real
    return (step_size, abar_re, abar_im, bbar_re, bbar_im)


def powers(decay_real, freq, step_size, length):
    steps_up = (jnp.arange(length, dtype=jnp.int32) + 1).astype(jnp.float32)[:, None, None]
    magnitude = jnp.exp((decay_real * step_size)[None] * steps_up)
    phase = (freq * step_size)[None] * steps_up
    return (magnitude * jnp.cos(phase), magnitude * jnp.sin(phase))


def compose(earlier, later):
    a1r, a1i, b1r, b1i = earlier
    a2r, a2i, b2r, b2i = later
    return (
        a2r * a1r - a2i * a1i,
        a2r * a1i + a2i * a1r,
        a2r * b1r - a2i * b1i + b2r,
        a2r * b1i + a2i * b1r + b2i,
    )


def local_states(inputs, decay_real, freq, step_size, bbar_re, bbar_im):
    highest = lax.Precision.DEFAULT
    tok_rows, group_count, unused = inputs.shape
    lanes = group_count * decay_real.shape[1]
    drive_re = jnp.einsum("lgm,gpm->lgp", inputs, bbar_re, precision=highest).reshape(
        tok_rows, lanes
    )
    drive_im = jnp.einsum("lgm,gpm->lgp", inputs, bbar_im, precision=highest).reshape(
        tok_rows, lanes
    )
    span = math.gcd(tok_rows, 16)
    spans = tok_rows // span
    rate = (decay_real * step_size).reshape(lanes)
    turn = (freq * step_size).reshape(lanes)
    later = jnp.arange(span, dtype=jnp.int32)[:, None]
    earlier = jnp.arange(span, dtype=jnp.int32)[None, :]
    lag = (later - earlier).astype(jnp.float32)
    causal = (later >= earlier)[..., None]
    lag_pos = jnp.maximum(lag, 0.0)[..., None]
    table_mag = jnp.exp(rate[None, None] * lag_pos)
    table_re = jnp.where(causal, table_mag * jnp.cos(turn[None, None] * lag_pos), 0.0)
    table_im = jnp.where(causal, table_mag * jnp.sin(turn[None, None] * lag_pos), 0.0)
    block_re = drive_re.reshape(spans, 1, span, lanes)
    block_im = drive_im.reshape(spans, 1, span, lanes)
    inner_re = jnp.sum(table_re[None] * block_re - table_im[None] * block_im, axis=2)
    inner_im = jnp.sum(table_re[None] * block_im + table_im[None] * block_re, axis=2)
    steps_up = (jnp.arange(span, dtype=jnp.int32) + 1).astype(jnp.float32)[:, None]
    pow_mag = jnp.exp(rate[None] * steps_up)
    pow_re = pow_mag * jnp.cos(turn[None] * steps_up)
    pow_im = pow_mag * jnp.sin(turn[None] * steps_up)
    span_re = pow_re[-1]
    span_im = pow_im[-1]

    def carry_step(entering, ends):
        next_re = span_re * entering[0] - span_im * entering[1] + ends[0]
        next_im = span_re * entering[1] + span_im * entering[0] + ends[1]
        return ((next_re, next_im), entering)

    zeros = jnp.zeros((lanes,), jnp.float32)
    unused_carry, entering = lax.scan(
        carry_step, (zeros, zeros), (inner_re[:, -1], inner_im[:, -1])
    )
    state_re = inner_re + pow_re[None] * entering[0][:, None] - pow_im[None] * entering[1][:, None]
    state_im = inner_im + pow_re[None] * entering[1][:, None] + pow_im[None] * entering[0][:, None]
    shape = (tok_rows, group_count, decay_real.shape[1])
    return (state_re.reshape(shape), state_im.reshape(shape))


def readout(state_re, state_im, out_real, out_imag, skip_mat, inputs):
    highest = lax.Precision.DEFAULT
    values = (
        jnp.einsum("lgp,gmp->lgm", state_re, out_real, precision=highest)
        - jnp.einsum("lgp,gmp->lgm", state_im, out_imag, precision=highest)
        + skip_mat[None] * inputs
    )
    values = jax.nn.gelu(values)
    return values.reshape(values.shape[0], -1).astype(jnp.bfloat16)


def row_norm(stream, norm_gain):
    scale_rows = lax.rsqrt(jnp.mean(stream * stream, axis=-1, keepdims=True) + EPS)
    return (stream * scale_rows * norm_gain).astype(jnp.bfloat16)


def per_device(
    ssm_input,
    residual_in,
    log_step,
    decay_real,
    freq,
    in_real,
    in_imag,
    out_real,
    out_imag,
    skip,
    w_glu,
    b_glu,
    w_branch,
    norm_gain,
    w_gate,
    w_up,
    w_down,
):
    tok_rows, width_local = ssm_input.shape
    group_count = log_step.shape[0]
    group_size = in_real.shape[2]
    tp_count = lax.axis_size("tp")
    tp_index = lax.axis_index("tp")
    own_rows = tok_rows // tp_count
    gate_whole, up_whole = sent_together((w_gate, w_up), SP, 0, 1)
    step_size, abar_re, abar_im, bbar_re, bbar_im = discretize(
        log_step, decay_real, freq, in_real, in_imag
    )
    pow_re, pow_im = powers(decay_real, freq, step_size, tok_rows)
    inputs = ssm_input.astype(jnp.float32).reshape(tok_rows, group_count, group_size)
    local_re, local_im = local_states(inputs, decay_real, freq, step_size, bbar_re, bbar_im)
    identity = (
        jnp.ones_like(abar_re),
        jnp.zeros_like(abar_re),
        jnp.zeros_like(abar_re),
        jnp.zeros_like(abar_re),
    )
    carried = entering_2(
        (pow_re[-1], pow_im[-1], local_re[-1], local_im[-1]), SP, compose, identity
    )
    state_re = local_re + pow_re * carried[2][None] - pow_im * carried[3][None]
    state_im = local_im + pow_re * carried[3][None] + pow_im * carried[2][None]
    mixer_out = readout(
        state_re, state_im, out_real, out_imag, skip.reshape(group_count, group_size), inputs
    )
    mixer_rows = lax.all_to_all(mixer_out, "tp", split_axis=0, concat_axis=1, tiled=True)
    glu_pre = jnp.dot(mixer_rows, w_glu, preferred_element_type=jnp.float32) + b_glu
    gated = (mixer_rows.astype(jnp.float32) * jax.nn.sigmoid(glu_pre)).astype(jnp.bfloat16)
    residual_own = lax.dynamic_slice_in_dim(residual_in, tp_index * own_rows, own_rows, 0)
    stream = residual_own.astype(jnp.float32) + jnp.dot(
        gated, w_branch, preferred_element_type=jnp.float32
    )
    normed = row_norm(stream, norm_gain)
    normed_all = gather_directly(normed, "tp", 0)
    gate_sum = jnp.dot(normed_all, gate_whole, preferred_element_type=jnp.float32)
    up_sum = jnp.dot(normed_all, up_whole, preferred_element_type=jnp.float32)
    hidden = (jax.nn.silu(gate_sum) * up_sum).astype(jnp.bfloat16)
    down_whole = lax.all_gather(w_down, SP, axis=1, tiled=True)
    summed = summed_on_arrival(
        jnp.dot(hidden, down_whole, preferred_element_type=jnp.float32).astype(jnp.bfloat16),
        "tp",
        0,
    )
    return (stream + summed).astype(jnp.bfloat16)


def solution(mesh):
    torus = Mesh(
        mesh.devices.reshape(mesh.shape["grp"], 16, 2, mesh.shape["tp"]),
        ("grp", "sp_0", "sp_1", "tp"),
    )
    in_specs = (
        P(GRP_SP, "tp"),
        P(GRP_SP, None),
        P("tp"),
        P("tp", None),
        P("tp", None),
        P("tp", None, None),
        P("tp", None, None),
        P("tp", None, None),
        P("tp", None, None),
        P("tp"),
        P(),
        P(),
        P(),
        P(),
        P(SP, "tp"),
        P(SP, "tp"),
        P("tp", SP),
    )
    out_specs = P(GRP_SP_TP, None)
    return jax.shard_map(
        per_device, mesh=torus, in_specs=in_specs, out_specs=out_specs, check_vma=False
    )
```

profile of v0, /device:TPU:33, one launch (start us, length us, event | category | flops | bytes accessed | tf_op | source)
XLA Modules:
  0.0 209.0 jit_solution(3152876637672829027)
XLA Ops:
  6.6 1.9 pad_maximum_fusion
  8.6 0.7 all-gather.7.cloned.1.call-update
  9.4 0.7 exp.36
  10.0 0.8 fusion.68
  11.0 0.9 copy.43
  12.0 5.8 %fusion.19 = (f32[16,16,1024]{2,1,0:T(8,128)}, f32[16,16,1024]{2,1,0:T(8,128)}) fusion(f32[1024]{0:T(1024)S(1)} %mul.861, f32[16,16]{1,0:T(8,128)S(1)} %convert_maximum_fusion, f32[1024]{0:T(1024)S(1)} %mul.856, pred[16,16]{1,0:T(8,128)(4,1)S(1)} %iota_compare_fusion), kind=kLoop, calls=%fused_computation.33 | loop fusion | flops 1572864 | bytes 2106624 | tf_op jit(solution)/shard_map/jit(_where)/select_n | solution.py:143
  17.8 2.0 convolution_bitcast_fusion.1
  19.8 2.0 convolution_bitcast_fusion
  21.8 1.5 copy.44
  23.4 1.1 mul.878
  24.5 1.5 copy.45
  26.1 1.1 mul.885
  27.2 6.3 %add_reduce_fusion = (f32[8,16,1024]{2,1,0:T(8,128)S(1)}, f32[8,16,1024]{2,1,0:T(8,128)S(1)}) fusion(f32[8,16,1024]{2,1,0:T(8,128)} %mul.885, f32[16,16,1024]{2,1,0:T(8,128)} %get-tuple-element.125, f32[8,16,1024]{2,1,0:T(8,128)} %mul.878, f32[16,16,1024]{2,1,0:T(8,128)} %get-tuple-element.124), kind=kLoop, calls=%fused_computation.6 | loop fusion | flops 16515072 | bytes 4194304 | tf_op jit(solution)/shard_map/reduce_sum | solution.py:148
  33.6 0.3 fusion.55
  34.0 12.5 %while.17 = (s32[]{:T(128)}, f32[1024]{0:T(1024)S(1)}, f32[1024]{0:T(1024)S(1)}, f32[8,1024]{1,0:T(8,128)S(1)}, f32[8,1024]{1,0:T(8,128)}, /*index=5*/f32[1024]{...) while((s32[]{:T(128)}, f32[1024]{0:T(1024)S(1)}, ...), condition=%wide.region_3.4_spmd.clone, body=%wide.region_2.3_spmd.clone.sunk | while | flops 10243 | bytes 90243 | solution.py:162
  34.0 0.1 dynamic_update_slice.11
  34.2 1.4 dynamic_update_slice.12
  35.6 0.1 dynamic_update_slice.11
  35.7 1.4 dynamic_update_slice.12
  37.2 0.1 dynamic_update_slice.11
  37.3 1.4 dynamic_update_slice.12
  38.7 0.1 dynamic_update_slice.11
  38.9 1.4 dynamic_update_slice.12
  40.4 1.4 dynamic_update_slice.12
  42.0 1.4 dynamic_update_slice.12
  43.5 1.4 dynamic_update_slice.12
  45.1 1.4 dynamic_update_slice.12
  46.5 1.9 multiply_add_fusion.1
  48.4 1.3 add.447
  49.8 2.3 %sub.173 = f32[128,16,64]{2,1,0:T(8,128)} reshape(f32[8,16,1024]{2,1,0:T(8,128)} %get-tuple-element.118) | data formatting | bytes 1048576 | tf_op jit(solution)/shard_map/sub | solution.py:165
  52.2 0.7 slice_bitcast_fusion.1
  52.9 3.9 %fusion.22 = (f32[128,16,64]{2,1,0:T(8,128)S(1)}, f32[128,16,64]{2,1,0:T(8,128)S(1)}) fusion(f32[16,64]{1,0:T(8,128)S(1)} %get-tuple-element.133, f32[128]{0:T(128)S(1)} %add_convert_fusion.1, f32[16,64]{1,0:T(8,128)S(1)} %get-tuple-element.132), kind=kLoop, calls=%fused_computation.36 | loop fusion | flops 524288 | bytes 1057280 | tf_op jit(solution)/shard_map/mul | solution.py:109
  56.8 22.0 %all-gather = f32[128,64]{1,0:T(8,128)S(1)} all-gather(f32[64,64]{1,0:T(8,128)S(1)} %pad_maximum_fusion.1), channel_id=2, replica_groups=mesh['grp'=2,'sp_0'=16,'sp_1'=2,'tp'=4] {'sp_1'}, dimensions={0}, use_global_device_ids=true | all-gather | bytes 49152 | tf_op jit(solution)/shard_map/all_gather | solution.py:37
  78.9 31.6 %all-gather.1 = f32[1024,64]{1,0:T(8,128)S(1)} all-gather(f32[64,64]{1,0:T(8,128)S(1)} %pad_maximum_fusion.2), channel_id=3, replica_groups=mesh['grp'=2,'sp_0'=16,'sp_1'=2,'tp'=4] {'sp_0'}, dimensions={0}, use_global_device_ids=true | all-gather | bytes 278528 | tf_op jit(solution)/shard_map/all_gather | solution.py:37
  110.6 6.7 %multiply_add_fusion = (bf16[128,16,64]{2,1,0:T(8,128)(2,1)S(1)}, bf16[128,16,64]{2,1,0:T(8,128)(2,1)S(1)}) fusion(f32[128,16,64]{2,1,0:T(8,128)S(1)} %add.447, f32[16,64]{1,0:T(8,128)S(1)} %add_bitcast_fusion, f32[16,64]{1,0:T(8,128)S(1)} %get-tuple-element.108, f32[16,64]{1,0:T(8,128)S(1)} %get-tuple-element.133, f32[128]{0:T(128)S(1)} %add_convert_fusion.1, ...), kind=kLoop, calls=%fused_computation.42 | loop fusion | flops 1835008 | bytes 1589760 | tf_op jit(solution)/shard_map/add | solution.py:229
  117.3 0.4 fusion.25
  117.7 1.3 fusion.44
  119.0 0.2 convert_element_type.64
  119.2 0.8 copy.48
  120.0 4.2 %all-to-all-start = ((bf16[4,32,256]{2,1,0:T(8,128)(2,1)}), bf16[4,32,256]{2,1,0:T(8,128)(2,1)S(1)}, u32[]{:S(2)}, u32[]{:S(2)}) async-start(bf16[4,32,256]{2,1,0:T(8,128)(2,1)} %copy.48), calls=%async_computation | async-start | bytes 131072 | tf_op jit(solution)/shard_map/all_to_all | solution.py:233
  124.2 4.5 %all-to-all-done = bf16[4,32,256]{2,1,0:T(8,128)(2,1)S(1)} async-done(((bf16[4,32,256]{2,1,0:T(8,128)(2,1)}), bf16[4,32,256]{2,1,0:T(8,128)(2,1)S(1)}, u32[]{:S(2)}, u32[]{:S(2)}) %all-to-all-start) | async-done | bytes 65568 | tf_op jit(solution)/shard_map/all_to_all | solution.py:233
  128.7 3.5 %multiply_reduce_fusion = (f32[32]{0:T(128)S(1)}, f32[32,2048]{1,0:T(8,128)S(1)}) fusion(bf16[1024,2048]{1,0:T(8,128)(2,1)} %param.31, bf16[32,1024]{1,0:T(8,128)(2,1)S(1)} %bitcast.174, bf16[1024,1024]{1,0:T(8,128)(2,1)S(1)} %copy-done, f32[1024]{0:T(1024)S(1)} %copy-done.3, bf16[128,2048]{1,0:T(8,128)(2,1)} %param.20, s32[]{:T(128)S(6)} %select_n.296), kind=kOutput, calls=%fused_computation.57 | convolution fusion | flops 201818080 | bytes 6819972 | tf_op jit(solution)/shard_map/dot_general | solution.py:237
  132.4 9.4 %all_to_all.26 = bf16[4,32,2048]{2,1,0:T(8,128)(2,1)S(1)} all-to-all(bf16[4,32,2048]{2,1,0:T(8,128)(2,1)S(1)} %broadcast_in_dim.32), channel_id=1, replica_groups=mesh['grp'=2,'sp_0'=16,'sp_1'=2,'tp'=4] {'tp'}, dimensions={0} | all-to-all | bytes 1048576 | tf_op jit(solution)/shard_map/all_to_all | solution.py:63
  141.8 4.6 %fusion.2 = f32[128,1408]{1,0:T(8,128)} fusion(bf16[128,2048]{1,0:T(8,128)(2,1)S(1)} %bitcast.167, bf16[2048,2816]{1,0:T(8,128)(2,1)} %all-gather.5.cloned.1.call-done), kind=kOutput, calls=%fused_computation.10 | convolution fusion | flops 738197504 | bytes 7012352 | tf_op jit(solution)/shard_map/dot_general | solution.py:242
  146.3 34.8 %all-gather.7.cloned.1.call-done = bf16[1408,2048]{0,1:T(8,128)(2,1)} async-done(((bf16[1408,64]{0,1:T(8,128)(2,1)}), bf16[1408,2048]{0,1:T(8,128)(2,1)}) %all-gather.7.cloned.1.call-update) | async-done | bytes 5767184 | tf_op jit(solution)/shard_map/all_gather | solution.py:245
  181.1 7.4 %convolution_convert_fusion = bf16[128,2048]{1,0:T(8,128)(2,1)S(1)} fusion(bf16[1408,2048]{0,1:T(8,128)(2,1)} %all-gather.7.cloned.1.call-done, bf16[128,2048]{1,0:T(8,128)(2,1)S(1)} %bitcast.168, bf16[2048,2816]{1,0:T(8,128)(2,1)} %all-gather.5.cloned.1.call-done, f32[128,1408]{1,0:T(8,128)} %fusion.2), kind=kOutput, calls=%fused_computation.14 | convolution fusion | flops 1477738496 | bytes 13303808 | tf_op jit(solution)/shard_map/dot_general | solution.py:247
  188.6 12.9 %all_to_all.27 = bf16[4,32,2048]{2,1,0:T(8,128)(2,1)S(1)} all-to-all(bf16[4,32,2048]{2,1,0:T(8,128)(2,1)S(1)} %bitcast.169), channel_id=1, replica_groups=mesh['grp'=2,'sp_0'=16,'sp_1'=2,'tp'=4] {'tp'}, dimensions={0} | all-to-all | bytes 1048576 | tf_op jit(solution)/shard_map/all_to_all | solution.py:87
  201.5 0.7 add_convert_fusion
  (71 shorter events, 1.5 us)
Async XLA Ops:
  6.5 122.1 %copy-start = (bf16[1024,1024]{1,0:T(8,128)(2,1)S(1)}, bf16[1024,1024]{1,0:T(8,128)(2,1)}, u32[]{:S(2)}) copy-start(bf16[1024,1024]{1,0:T(8,128)(2,1)} %param.29) | copy-start | bytes 6291460
  6.6 135.2 %all-gather.5.cloned.1.call-start = ((), (), s32[]{:S(2)}) async-start(), calls=%async_computation.3 | async-start | bytes 11894784 | tf_op jit(solution)/shard_map/all_gather | solution.py:20
  8.5 172.6 %all-gather.7.cloned.1.call-start = ((), (), s32[]{:S(2)}) async-start(), calls=%async_computation.4 | async-start | bytes 5947392 | tf_op jit(solution)/shard_map/all_gather | solution.py:245
  27.2 24.9 %copy-start.4 = (f32[256]{0:T(256)S(1)}, f32[256]{0:T(256)}, u32[]{:S(2)}) copy-start(f32[256]{0:T(256)} %param.28) | copy-start | bytes 3076
  46.5 70.8 %copy-start.1 = (f32[16,16,64]{2,1,0:T(8,128)S(1)}, f32[16,16,64]{2,1,0:T(8,128)}, u32[]{:S(2)}) copy-start(f32[16,16,64]{2,1,0:T(8,128)} %param.26) | copy-start | bytes 196612
  49.8 78.9 %copy-start.3 = (f32[1024]{0:T(1024)S(1)}, f32[1024]{0:T(1024)}, u32[]{:S(2)}) copy-start(f32[1024]{0:T(1024)} %param.30) | copy-start | bytes 12292
  110.6 21.7 %copy-start.2 = (f32[2048]{0:T(1024)S(1)}, f32[2048]{0:T(1024)}, u32[]{:S(2)}) copy-start(f32[2048]{0:T(1024)} %param.32) | copy-start | bytes 24580
  120.0 8.7 %all-to-all-start = ((bf16[4,32,256]{2,1,0:T(8,128)(2,1)}), bf16[4,32,256]{2,1,0:T(8,128)(2,1)S(1)}, u32[]{:S(2)}, u32[]{:S(2)}) async-start(bf16[4,32,256]{2,1,0:T(8,128)(2,1)} %copy.48), calls=%async_computation | async-start | bytes 131072 | tf_op jit(solution)/shard_map/all_to_all | solution.py:233
Sparse Core Ops, SparseCore 0:
  9.2 101.0 all-gather.4
  112.1 68.9 all-gather.6
where the time goes:
time: 210 us; the launch traced here: 209 us
  blocking collectives  75.9 us (36%)
  waiting for transfers between devices  40.1 us (19%)
  other arithmetic  28.9 us (14%)
  local copies, waits for them, and re-layouts  24.7 us (12%)
  matrix products  21.3 us (10%)
  between operations  13.7 us (7%)
  starting transfers between devices  4.27 us (2%)
    all_gather x2, blocking collectives, all_in_one(): both, at, found = (lax.all_gather(jnp.concatenate(lines), axis), 0, {})  53.6 us
    all_gather x1, waiting for transfers between devices, per_device(): down_whole = lax.all_gather(w_down, SP, axis=1, tiled=True)  34.8 us
    all_to_all x1, blocking collectives, summed_on_arrival(): lax.all_to_all(pieces, axis, split_axis=0, concat_axis=0, tiled=True)  12.9 us
    dynamic_update_slice x16, local copies, waits for them, and re-layouts, local_states(): lax.scan(carry_step, (zeros, zeros), (inner_re[:, -1], inner_im[:, -1]))  12.1 us
    all_to_all x1, blocking collectives, sent_to_all(): lax.all_to_all(jnp.broadcast_to(shard[None], (count, *shard.shape)), axis...  9.36 us
    dot_general x1, matrix products, per_device(): jnp.dot(hidden, down_whole, preferred_element_type=jnp.float32)  7.42 us
    add x1, other arithmetic, per_device(): state_im = local_im + pow_re * carried[3][None] + pow_im * carried[2][None]  6.71 us
    reduce_sum x1, other arithmetic, local_states(): jnp.sum(table_re[None] * block_im + table_im[None] * block_re, axis=2)  6.35 us
  transfers between devices with their start and end apart: 3, of which 2 were waited for; matrix products, arithmetic and copies ran while one was open for 31% of the time, Pallas kernels for 0%

commit v1 on v0

--- a/solution.py
+++ b/solution.py
@@ -242,7 +242,9 @@
     gate_sum = jnp.dot(normed_all, gate_whole, preferred_element_type=jnp.float32)
     up_sum = jnp.dot(normed_all, up_whole, preferred_element_type=jnp.float32)
     hidden = (jax.nn.silu(gate_sum) * up_sum).astype(jnp.bfloat16)
-    down_whole = lax.all_gather(w_down, SP, axis=1, tiled=True)
+    down_whole = jnp.concatenate(
+        lax.all_to_all(jnp.stack([w_down] * lax.axis_size(SP)), SP, 0, 0), axis=1
+    )
     summed = summed_on_arrival(
         jnp.dot(hidden, down_whole, preferred_element_type=jnp.float32).astype(jnp.bfloat16),
         "tp",

time: 210 us -> 490 us (2.33)
  waiting for transfers between devices: 40.1 us -> 295 us
  starting transfers between devices: 4.27 us -> 19.3 us
  local copies, waits for them, and re-layouts: 24.7 us -> 38.3 us
    all_gather x1, waiting for transfers between devices: 0.01 us -> 230 us  [sent_together(): lax.all_gather(both, axis, axis=dim, tiled=True)]
    all_to_all x0 -> x1, waiting for transfers between devices: none -> 61.5 us  [per_device(): lax.all_to_all(jnp.stack([w_down] * lax.axis_size(SP)), SP, 0, 0)]
    all_gather x1 -> x0, waiting for transfers between devices: 34.8 us -> none  [per_device(): down_whole = lax.all_gather(w_down, SP, axis=1, tiled=True)]
    all_to_all x0 -> x1, starting transfers between devices: none -> 15 us  [per_device(): lax.all_to_all(jnp.stack([w_down] * lax.axis_size(SP)), SP, 0, 0)]
    dynamic_update_slice x16, local copies, waits for them, and re-layouts: 12.1 us -> 22.3 us  [local_states(): lax.scan(carry_step, (zeros, zeros), (inner_re[:, -1], inner_im[:, -1]))]
  transfers between devices with their start and end apart: 3 -> 3, of which waited for: 2 -> 3; matrix products, arithmetic and copies ran while one was open for 31% -> 3% of each run, Pallas kernels for 0% -> 0%
where the time goes in v1:
time: 490 us; the launch traced here: 488 us
  waiting for transfers between devices  295 us (60%)
  blocking collectives  71.4 us (15%)
  local copies, waits for them, and re-layouts  38.3 us (8%)
  other arithmetic  27.8 us (6%)
  matrix products  22.2 us (5%)
  starting transfers between devices  19.3 us (4%)
  between operations  13.7 us (3%)
    all_gather x1, waiting for transfers between devices, sent_together(): lax.all_gather(both, axis, axis=dim, tiled=True)  230 us
    all_to_all x1, waiting for transfers between devices, per_device(): lax.all_to_all(jnp.stack([w_down] * lax.axis_size(SP)), SP, 0, 0)  61.5 us
    all_gather x2, blocking collectives, all_in_one(): both, at, found = (lax.all_gather(jnp.concatenate(lines), axis), 0, {})  49.5 us
    dynamic_update_slice x16, local copies, waits for them, and re-layouts, local_states(): lax.scan(carry_step, (zeros, zeros), (inner_re[:, -1], inner_im[:, -1]))  22.3 us
    all_to_all x1, starting transfers between devices, per_device(): lax.all_to_all(jnp.stack([w_down] * lax.axis_size(SP)), SP, 0, 0)  15 us
    all_to_all x1, blocking collectives, summed_on_arrival(): lax.all_to_all(pieces, axis, split_axis=0, concat_axis=0, tiled=True)  12.5 us
  transfers between devices with their start and end apart: 3, of which 3 were waited for; matrix products, arithmetic and copies ran while one was open for 3% of the time, Pallas kernels for 0%

profile of v1, /device:TPU:33, one launch (start us, length us, event | category | flops | bytes accessed | tf_op | source)
XLA Modules:
  0.0 487.5 jit_solution(12552247322019096665)
XLA Ops:
  6.6 1.1 copy.44
  9.2 2.0 convolution_bitcast_fusion
  11.2 2.0 convolution_bitcast_fusion.1
  13.3 1.5 copy.46
  14.8 1.1 mul.885
  16.1 1.5 copy.45
  17.6 1.1 mul.878
  19.1 4.0 fusion.19
  23.1 6.2 %add_reduce_fusion = (f32[8,16,1024]{2,1,0:T(8,128)S(1)}, f32[8,16,1024]{2,1,0:T(8,128)S(1)}) fusion(f32[8,16,1024]{2,1,0:T(8,128)} %mul.885, f32[16,16,1024]{2,1,0:T(8,128)S(1)} %get-tuple-element.125, f32[8,16,1024]{2,1,0:T(8,128)} %mul.878, f32[16,16,1024]{2,1,0:T(8,128)S(1)} %get-tuple-element.124), kind=kLoop, calls=%fused_computation.6 | loop fusion | flops 16515072 | bytes 4194304 | tf_op jit(solution)/shard_map/reduce_sum | solution.py:148
  29.4 22.7 %while.17 = (s32[]{:T(128)}, f32[1024]{0:T(1024)S(1)}, f32[1024]{0:T(1024)S(1)}, f32[8,1024]{1,0:T(8,128)}, f32[8,1024]{1,0:T(8,128)}, /*index=5*/f32[1024]{0:T(...) while((s32[]{:T(128)}, f32[1024]{0:T(1024)S(1)}, ...), condition=%wide.region_3.4_spmd.clone, body=%wide.region_2.3_spmd.clone.sunk | while | flops 10243 | bytes 90251 | solution.py:162
  29.5 1.4 dynamic_update_slice.11
  30.9 1.4 dynamic_update_slice.12
  32.3 1.4 dynamic_update_slice.11
  33.7 1.4 dynamic_update_slice.12
  35.1 1.4 dynamic_update_slice.11
  36.5 1.4 dynamic_update_slice.12
  38.0 1.4 dynamic_update_slice.11
  39.4 1.4 dynamic_update_slice.12
  40.8 1.4 dynamic_update_slice.11
  42.2 1.4 dynamic_update_slice.12
  43.6 1.4 dynamic_update_slice.11
  45.0 1.4 dynamic_update_slice.12
  46.5 1.4 dynamic_update_slice.11
  47.9 1.4 dynamic_update_slice.12
  49.3 1.4 dynamic_update_slice.11
  50.7 1.4 dynamic_update_slice.12
  52.1 1.9 multiply_add_fusion.1
  54.0 1.3 add.447
  55.3 2.3 sub.173
  58.4 3.9 fusion.22
  62.3 22.0 %all-gather = f32[128,64]{1,0:T(8,128)S(1)} all-gather(f32[64,64]{1,0:T(8,128)S(1)} %pad_maximum_fusion.1), channel_id=2, replica_groups=mesh['grp'=2,'sp_0'=16,'sp_1'=2,'tp'=4] {'sp_1'}, dimensions={0}, use_global_device_ids=true | all-gather | bytes 49152 | tf_op jit(solution)/shard_map/all_gather | solution.py:37
  84.3 27.6 %all-gather.1 = f32[1024,64]{1,0:T(8,128)} all-gather(f32[64,64]{1,0:T(8,128)S(1)} %pad_maximum_fusion.2), channel_id=3, replica_groups=mesh['grp'=2,'sp_0'=16,'sp_1'=2,'tp'=4] {'sp_0'}, dimensions={0}, use_global_device_ids=true | all-gather | bytes 278528 | tf_op jit(solution)/shard_map/all_gather | solution.py:37
  112.0 1.2 add_bitcast_fusion.1
  113.2 6.7 %multiply_add_fusion = (bf16[128,16,64]{2,1,0:T(8,128)(2,1)S(1)}, bf16[128,16,64]{2,1,0:T(8,128)(2,1)S(1)}) fusion(f32[128,16,64]{2,1,0:T(8,128)S(1)} %add.447, f32[16,64]{1,0:T(8,128)S(1)} %add_bitcast_fusion, f32[16,64]{1,0:T(8,128)S(1)} %get-tuple-element.108, f32[16,64]{1,0:T(8,128)S(1)} %get-tuple-element.133, f32[128]{0:T(128)S(1)} %add_convert_fusion.1, ...), kind=kLoop, calls=%fused_computation.42 | loop fusion | flops 1835008 | bytes 1589760 | tf_op jit(solution)/shard_map/add | solution.py:229
  119.9 1.3 fusion.25
  121.2 1.4 fusion.44
  123.5 4.3 all-to-all-start
  127.8 1.7 pad_maximum_fusion
  129.6 2.7 all-to-all-done
  132.3 3.5 multiply_reduce_fusion
  136.0 9.4 %all_to_all.31 = bf16[4,32,2048]{2,1,0:T(8,128)(2,1)S(1)} all-to-all(bf16[4,32,2048]{2,1,0:T(8,128)(2,1)S(1)} %broadcast_in_dim.32), channel_id=1, replica_groups=mesh['grp'=2,'sp_0'=16,'sp_1'=2,'tp'=4] {'tp'}, dimensions={0} | all-to-all | bytes 1048576 | tf_op jit(solution)/shard_map/all_to_all | solution.py:63
  145.4 3.2 stack.2
  148.6 15.0 %all-to-all-start.2 = ((bf16[32,1408,64]{1,2,0:T(8,128)(2,1)}), bf16[32,1408,64]{1,2,0:T(8,128)(2,1)}, u32[]{:S(2)}, u32[]{:S(2)}) async-start(bf16[32,1408,64]{1,2,0:T(8,128)(2,1)} %stack.2), calls=%async_computation.2 | async-start | bytes 11534336 | tf_op jit(solution)/shard_map/all_to_all | solution.py:246
  163.6 230.3 %all-gather.4.cloned.1.call-done = bf16[2048,2816]{1,0:T(8,128)(2,1)} async-done(((bf16[64,2816]{1,0:T(8,128)(2,1)}), bf16[2048,2816]{1,0:T(8,128)(2,1)}) %all-gather.4.cloned.1.call-update) | async-done | bytes 11534352 | tf_op jit(solution)/shard_map/all_gather | solution.py:20
  393.9 4.6 fusion.2
  398.5 61.5 %all-to-all-done.2 = bf16[32,1408,64]{1,2,0:T(8,128)(2,1)} async-done(((bf16[32,1408,64]{1,2,0:T(8,128)(2,1)}), bf16[32,1408,64]{1,2,0:T(8,128)(2,1)}, u32[]{:S(2)}, u32[]{:S(2)}) %all-to-all-start.2) | async-done | bytes 5767200 | tf_op jit(solution)/shard_map/all_to_all | solution.py:246
  460.0 7.4 %convolution_convert_fusion = bf16[128,2048]{1,0:T(8,128)(2,1)S(1)} fusion(bf16[1408,2048]{0,1:T(8,128)(2,1)} %bitcast.25, bf16[128,2048]{1,0:T(8,128)(2,1)S(1)} %bitcast.171, bf16[2048,2816]{1,0:T(8,128)(2,1)} %all-gather.4.cloned.1.call-done, f32[128,1408]{1,0:T(8,128)} %fusion.2), kind=kOutput, calls=%fused_computation.14 | convolution fusion | flops 1477738496 | bytes 13303808 | tf_op jit(solution)/shard_map/dot_general | solution.py:249
  467.4 12.5 %all_to_all.32 = bf16[4,32,2048]{2,1,0:T(8,128)(2,1)S(1)} all-to-all(bf16[4,32,2048]{2,1,0:T(8,128)(2,1)S(1)} %bitcast.172), channel_id=1, replica_groups=mesh['grp'=2,'sp_0'=16,'sp_1'=2,'tp'=4] {'tp'}, dimensions={0} | all-to-all | bytes 1048576 | tf_op jit(solution)/shard_map/all_to_all | solution.py:87
  (73 shorter events, 5.1 us)
Async XLA Ops:
  6.5 125.8 %copy-start = (bf16[1024,1024]{1,0:T(8,128)(2,1)S(1)}, bf16[1024,1024]{1,0:T(8,128)(2,1)}, u32[]{:S(2)}) copy-start(bf16[1024,1024]{1,0:T(8,128)(2,1)} %param.29) | copy-start | bytes 6291460
  29.3 82.6 %copy-start.5 = (f32[256]{0:T(256)S(1)}, f32[256]{0:T(256)}, u32[]{:S(2)}) copy-start(f32[256]{0:T(256)} %param.28) | copy-start | bytes 3076
  55.3 72.5 %copy-start.2 = (bf16[64,1408]{1,0:T(8,128)(2,1)S(1)}, bf16[64,1408]{1,0:T(8,128)(2,1)}, u32[]{:S(2)}) copy-start(bf16[64,1408]{1,0:T(8,128)(2,1)} %param.34) | copy-start | bytes 540676
  57.7 74.6 %copy-start.4 = (f32[1024]{0:T(1024)S(1)}, f32[1024]{0:T(1024)}, u32[]{:S(2)}) copy-start(f32[1024]{0:T(1024)} %param.30) | copy-start | bytes 12292
  119.9 15.9 %copy-start.3 = (f32[2048]{0:T(1024)S(1)}, f32[2048]{0:T(1024)}, u32[]{:S(2)}) copy-start(f32[2048]{0:T(1024)} %param.32) | copy-start | bytes 24580
  121.2 24.2 %copy-start.1 = (bf16[1408,64]{0,1:T(8,128)(2,1)S(1)}, bf16[1408,64]{0,1:T(8,128)(2,1)}, u32[]{:S(2)}) copy-start(bf16[1408,64]{0,1:T(8,128)(2,1)} %param.35) | copy-start | bytes 540676
  123.5 8.8 %all-to-all-start = ((bf16[4,32,256]{2,1,0:T(8,128)(2,1)}), bf16[4,32,256]{2,1,0:T(8,128)(2,1)S(1)}, u32[]{:S(2)}, u32[]{:S(2)}) async-start(bf16[4,32,256]{2,1,0:T(8,128)(2,1)} %copy.49), calls=%async_computation | async-start | bytes 131072 | tf_op jit(solution)/shard_map/all_to_all | solution.py:233
  127.8 266.1 %all-gather.4.cloned.1.call-start = ((), (), s32[]{:S(2)}) async-start(), calls=%async_computation.4 | async-start | bytes 11894784 | tf_op jit(solution)/shard_map/all_gather | solution.py:20
  148.6 311.4 %all-to-all-start.2 = ((bf16[32,1408,64]{1,2,0:T(8,128)(2,1)}), bf16[32,1408,64]{1,2,0:T(8,128)(2,1)}, u32[]{:S(2)}, u32[]{:S(2)}) async-start(bf16[32,1408,64]{1,2,0:T(8,128)(2,1)} %stack.2), calls=%async_computation.2 | async-start | bytes 11534336 | tf_op jit(solution)/shard_map/all_to_all | solution.py:246
Sparse Core Ops, SparseCore 0:
  130.5 263.4 all-gather.3
